TPU v7x, 32 devices: a whole 2x2x4 slice. The times are simulated.
32 devices in a mesh: sp: 8 (over z, y), tp: 4 (over x, core).
Axes of the slice: x: 2, y: 2, z: 4, core: 2. Of those that a mesh axis runs over, the one named last changes fastest.
Arguments:
- queries: bfloat16 [4096, 2048], P('sp', 'tp'), may hold values from -6 to 6
- keys: bfloat16 [4096, 512], P('sp', 'tp'), may hold values from -6 to 6
- values: bfloat16 [4096, 512], P('sp', 'tp'), may hold values from -6 to 6
- residual: bfloat16 [4096, 2048], P(('sp', 'tp')), may hold values from -0.119628906 to 0.119628906
- out_proj: bfloat16 [2048, 2048], replicated, may hold values from -0.125 to 0.125
- query_gain: float32 [128], replicated, may hold values from 0.7 to 7
- key_gain: float32 [128], replicated, may hold values from 0.7 to 7
- norm_gain: float32 [2048], replicated, may hold values from 0.1 to 1.9
- routes: int32 [4096, 4], P(('sp', 'tp')), may hold values from 0 to 31, all different within a row; in each aligned block of 128 rows (0 to 127, 128 to 255, ...) at most 32 rows name the same one
- route_weight: float32 [4096, 4], P(('sp', 'tp')), may hold values from 0.1 to 1
- expert_gate: bfloat16 [32, 2048, 256], P(('sp', 'tp')), may hold values from -0.125 to 0.125
- expert_up: bfloat16 [32, 2048, 256], P(('sp', 'tp')), may hold values from -0.125 to 0.125
- expert_down: bfloat16 [32, 256, 2048], P(('sp', 'tp')), may hold values from -0.375 to 0.375
- shared_gate: bfloat16 [2048, 256], replicated, may hold values from -0.125 to 0.125
- shared_up: bfloat16 [2048, 256], replicated, may hold values from -0.125 to 0.125
- shared_down: bfloat16 [256, 2048], replicated, may hold values from -0.375 to 0.375
Outputs:
- layer_out: bfloat16 [4096, 2048], P(('sp', 'tp'))
Inputs may be any that keep to these rules, and one draw needn't show every extreme that they name: In the rows of one device (aligned blocks of 128 tokens), no expert is named by more than 32 routes; some expert is named by exactly 32 routes of some device; the 4 experts of a token differ.
All inputs are finite; a program needn't handle non-finite values.
Results may differ from a plain program's by a relative error of at most 0.023.
The roundings to bfloat16 on the way count: a program that leaves them out, or rounds other values in their place, can miss the bound.
Values may be sent and summed in bfloat16 or wider, within the bound.
A program may use at most 128 MiB of HBM per device.

v0:
```python
import math
import jax
import jax.numpy as jnp
from jax import lax
from jax.sharding import PartitionSpec as P

HEADS = 16
KV_HEADS = 4
GRID_W = 64
EPS = 1e-06
THETA = 10000.0


def rotate_pairs(block, cosine, sine):
    first, second = jnp.split(block, 2, axis=-1)
    return jnp.concatenate(
        [first * cosine - second * sine, second * cosine + first * sine], axis=-1
    )


def normed_rotary(source, gain, heads, offset):
    count = source.shape[0]
    width = gain.shape[0]
    values_f = source.astype(jnp.float32).reshape(count, heads, width)
    values_f = (
        values_f * lax.rsqrt(jnp.mean(values_f * values_f, axis=-1, keepdims=True) + EPS) * gain
    )
    position = offset + jnp.arange(count, dtype=jnp.int32)
    grid_row = (position // GRID_W).astype(jnp.float32)
    grid_col = (position % GRID_W).astype(jnp.float32)
    quarter = width // 4
    inverse = jnp.power(THETA, -4.0 * jnp.arange(quarter, dtype=jnp.float32) / width)
    row_angle = (grid_row[:, None] * inverse[None, :])[:, None, :]
    col_angle = (grid_col[:, None] * inverse[None, :])[:, None, :]
    row_half, col_half = jnp.split(values_f, 2, axis=-1)
    turned = jnp.concatenate(
        [
            rotate_pairs(row_half, jnp.cos(row_angle), jnp.sin(row_angle)),
            rotate_pairs(col_half, jnp.cos(col_angle), jnp.sin(col_angle)),
        ],
        axis=-1,
    )
    return turned.reshape(count, heads * width).astype(jnp.bfloat16)


def expert_apply(arrived, expert_gate, expert_up, expert_down):
    sources, slots, width = arrived.shape
    local = expert_gate.shape[0]
    grouped = arrived.reshape(sources // local, local, slots, width)
    gate_part = jnp.einsum(
        "sech,ehf->secf", grouped, expert_gate, preferred_element_type=jnp.float32
    )
    up_part = jnp.einsum("sech,ehf->secf", grouped, expert_up, preferred_element_type=jnp.float32)
    hidden_e = (jax.nn.silu(gate_part) * up_part).astype(jnp.bfloat16)
    result = jnp.einsum("secf,efh->sech", hidden_e, expert_down, preferred_element_type=jnp.float32)
    return result.astype(jnp.bfloat16).reshape(sources, slots, width)


def body(
    queries,
    keys,
    values,
    residual,
    out_proj,
    query_gain,
    key_gain,
    norm_gain,
    routes,
    route_weight,
    expert_gate,
    expert_up,
    expert_down,
    shared_gate,
    shared_up,
    shared_down,
):
    tok_local = queries.shape[0]
    width = query_gain.shape[0]
    group = HEADS // KV_HEADS
    kv_local = keys.shape[1] // width
    scale = 1.0 / math.sqrt(width)
    offset = lax.axis_index("sp") * tok_local
    q_rot = normed_rotary(queries, query_gain, kv_local * group, offset)
    k_rot = normed_rotary(keys, key_gain, kv_local, offset)
    query_3d = q_rot.reshape(tok_local, kv_local, group, width).transpose(1, 2, 0, 3)
    query_3d = query_3d.reshape(kv_local, group * tok_local, width)
    start_state = (
        jnp.full((kv_local, group * tok_local), -jnp.inf, jnp.float32),
        jnp.zeros((kv_local, group * tok_local), jnp.float32),
        jnp.zeros((kv_local, group * tok_local, width), jnp.float32),
    )
    key_piece = lax.all_gather(k_rot, "sp", axis=0, tiled=True)
    value_piece = lax.all_gather(values, "sp", axis=0, tiled=True)
    count = key_piece.shape[0]
    block = math.gcd(count, 512)

    def one_block(index_block, state):
        running_max, running_sum, accum = state
        key_rows = lax.dynamic_slice_in_dim(key_piece, index_block * block, block, 0)
        value_rows = lax.dynamic_slice_in_dim(value_piece, index_block * block, block, 0)
        key_3d = key_rows.reshape(block, kv_local, width)
        value_3d = value_rows.reshape(block, kv_local, width)
        scores = (
            jnp.einsum("gqd,kgd->gqk", query_3d, key_3d, preferred_element_type=jnp.float32) * scale
        )
        new_max = jnp.maximum(running_max, jnp.max(scores, axis=-1))
        weights = jnp.exp(scores - new_max[..., None])
        factor = jnp.exp(running_max - new_max)
        new_sum = running_sum * factor + jnp.sum(weights, axis=-1)
        added = jnp.einsum(
            "gqk,kgd->gqd",
            weights.astype(jnp.bfloat16),
            value_3d,
            preferred_element_type=jnp.float32,
        )
        return (new_max, new_sum, accum * factor[..., None] + added)

    final_max, final_sum, final_acc = lax.fori_loop(0, count // block, one_block, start_state)
    attn_local = (final_acc / final_sum[..., None]).astype(jnp.bfloat16)
    attn_local = attn_local.reshape(kv_local, group, tok_local, width).transpose(2, 0, 1, 3)
    attn_local = attn_local.reshape(tok_local, kv_local * group * width)
    all_heads = lax.all_to_all(attn_local, "tp", split_axis=0, concat_axis=1, tiled=True)
    projected = jnp.dot(all_heads, out_proj, preferred_element_type=jnp.float32)
    hidden1 = (residual.astype(jnp.float32) + projected).astype(jnp.bfloat16)
    hidden_f = hidden1.astype(jnp.float32)
    normed = (
        hidden_f
        * lax.rsqrt(jnp.mean(hidden_f * hidden_f, axis=-1, keepdims=True) + EPS)
        * norm_gain
    ).astype(jnp.bfloat16)
    rows_local = normed.shape[0]
    top_count = routes.shape[1]
    pair_count = rows_local * top_count
    expert_total = expert_gate.shape[0] * lax.axis_size("sp") * lax.axis_size("tp")
    capacity = max(2, 2 * rows_local * top_count // expert_total)
    flat_routes = routes.reshape(pair_count)
    one_hot = (flat_routes[:, None] == jnp.arange(expert_total, dtype=jnp.int32)[None, :]).astype(
        jnp.float32
    )
    lower = (jnp.arange(pair_count)[:, None] >= jnp.arange(pair_count)[None, :]).astype(jnp.float32)
    running_count = jnp.dot(lower, one_hot, precision=lax.Precision.HIGHEST)
    slot_place = (jnp.sum(running_count * one_hot, axis=1) - 1.0).astype(jnp.int32)
    slot_index = flat_routes * capacity + slot_place
    slot_total = expert_total * capacity
    placement = (jnp.arange(slot_total, dtype=jnp.int32)[:, None] == slot_index[None, :]).astype(
        jnp.bfloat16
    )
    placement = jnp.sum(placement.reshape(slot_total, rows_local, top_count), axis=2)
    send_rows = jnp.dot(placement, normed, preferred_element_type=jnp.float32).astype(jnp.bfloat16)
    send_rows = send_rows.reshape(expert_total, capacity, normed.shape[1])
    shared_hidden = (
        jax.nn.silu(jnp.dot(normed, shared_gate, preferred_element_type=jnp.float32))
        * jnp.dot(normed, shared_up, preferred_element_type=jnp.float32)
    ).astype(jnp.bfloat16)
    shared_out = jnp.dot(shared_hidden, shared_down, preferred_element_type=jnp.float32)
    processed = expert_apply(
        lax.all_to_all(send_rows, ("sp", "tp"), split_axis=0, concat_axis=0, tiled=True),
        expert_gate,
        expert_up,
        expert_down,
    )
    returned = lax.all_to_all(processed, ("sp", "tp"), split_axis=0, concat_axis=0, tiled=True)
    returned = returned.reshape(slot_total, normed.shape[1])
    routed = (
        returned[slot_index].reshape(rows_local, top_count, normed.shape[1]).astype(jnp.float32)
    )
    mixed = jnp.einsum("tk,tkd->td", route_weight, routed) + shared_out
    return (hidden_f + mixed).astype(jnp.bfloat16)


def solution(mesh):
    placed = (
        P("sp", "tp"),
        P("sp", "tp"),
        P("sp", "tp"),
        P(("sp", "tp"), None),
        P(),
        P(),
        P(),
        P(),
        P(("sp", "tp"), None),
        P(("sp", "tp"), None),
        P(("sp", "tp"), None, None),
        P(("sp", "tp"), None, None),
        P(("sp", "tp"), None, None),
        P(),
        P(),
        P(),
    )
    return jax.shard_map(
        body, mesh=mesh, in_specs=placed, out_specs=P(("sp", "tp"), None), check_vma=False
    )
```

profile of v0, /device:TPU:0, one launch (start us, length us, event | category | flops | bytes accessed | tf_op | source)
XLA Modules:
  0.0 420.8 jit_solution(3090994777994951920)
XLA Ops:
  6.6 1.1 copy.35
  7.7 0.7 fusion.43
  8.5 0.6 fusion.62
  9.0 0.7 pad_maximum_fusion
  9.8 0.7 all-gather.4.cloned.1.call-update
  10.5 1.4 reshape.480
  11.9 0.6 multiply_reduce_fusion.2
  12.6 1.9 multiply_cosine_fusion.1
  14.5 0.7 multiply_multiply_fusion
  15.2 1.8 fusion.37
  17.0 1.6 maximum_bitcast_fusion
  19.2 32.9 %all-gather.6.cloned.1.call-done = bf16[4096,1,128]{0,2,1:T(8,128)(2,1)} async-done(((bf16[512,1,128]{0,2,1:T(8,128)(2,1)}), bf16[4096,1,128]{0,2,1:T(8,128)(2,1)}) %all-gather.6.cloned.1.call-update) | async-done | bytes 1048592 | tf_op jit(solution)/shard_map/all_gather | solution.py:92
  52.1 41.4 %all-gather.4.cloned.1.call-done = bf16[4096,128]{1,0:T(8,128)(2,1)} async-done(((bf16[512,128]{1,0:T(8,128)(2,1)}), bf16[4096,128]{1,0:T(8,128)(2,1)}) %all-gather.4.cloned.1.call-update) | async-done | bytes 1048592 | tf_op jit(solution)/shard_map/all_gather | solution.py:93
  93.6 73.7 %while.18 = (s32[]{:T(128)}, f32[1,2048]{1,0:T(1,128)S(1)}, f32[1,2048]{1,0:T(1,128)S(1)}, f32[1,2048,128]{2,1,0:T(8,128)S(1)}, bf16[4096,128]{0,1:T(8,128)(2,1)...) while((s32[]{:T(128)}, f32[1,2048]{1,0:T(1,128)S(1)}, ...), condition=%wide.region_5.6_spmd.clone, body=%wide.region_2.5_spmd.clone.sunk | while | flops 546056192 | bytes 32374984 | solution.py:118
  93.6 3.6 multiply_reduce_fusion.4
  97.2 3.0 fusion.96
  100.3 0.3 copy-done.1
  100.6 2.1 fusion.98
  102.8 3.6 multiply_reduce_fusion.4
  106.4 3.0 fusion.96
  109.5 0.3 copy-done.1
  109.8 2.1 fusion.98
  112.0 3.6 multiply_reduce_fusion.4
  115.6 3.0 fusion.96
  118.7 0.3 copy-done.1
  119.0 2.1 fusion.98
  121.2 3.6 multiply_reduce_fusion.4
  124.8 3.0 fusion.96
  127.9 0.3 copy-done.1
  128.3 2.1 fusion.98
  130.4 3.6 multiply_reduce_fusion.4
  134.1 3.0 fusion.96
  137.1 0.3 copy-done.1
  137.5 2.1 fusion.98
  139.7 3.6 multiply_reduce_fusion.4
  143.3 3.0 fusion.96
  146.4 0.3 copy-done.1
  146.7 2.1 fusion.98
  148.9 3.6 multiply_reduce_fusion.4
  152.5 3.0 fusion.96
  155.6 0.3 copy-done.1
  155.9 2.1 fusion.98
  158.1 3.6 multiply_reduce_fusion.4
  161.7 3.0 fusion.96
  164.8 0.3 copy-done.1
  165.2 2.1 fusion.98
  167.3 0.3 divide_convert_fusion
  167.7 0.4 copy.51
  168.1 1.0 all_to_all.20
  169.1 3.7 all-to-all-start
  173.2 8.1 %all-to-all-done = bf16[4,128,512]{2,1,0:T(8,128)(2,1)S(1)} async-done(((bf16[4,128,512]{2,1,0:T(8,128)(2,1)}), bf16[4,128,512]{2,1,0:T(8,128)(2,1)S(1)}, u32[]{:S(2)}, u32[]{:S(2)}) %all-to-all-start) | async-done | bytes 524320 | tf_op jit(solution)/shard_map/all_to_all | solution.py:122
  181.6 4.7 %multiply_reduce_fusion.1 = (f32[128]{0:T(128)S(1)}, f32[128,2048]{1,0:T(8,128)S(1)}) fusion(bf16[128,2048]{0,1:T(8,128)(2,1)S(1)} %bitcast.106, bf16[2048,2048]{1,0:T(8,128)(2,1)} %param.22, bf16[128,2048]{1,0:T(8,128)(2,1)S(1)} %copy-done.5), kind=kOutput, calls=%fused_computation.52 | convolution fusion | flops 1075314560 | bytes 10486272 | tf_op jit(solution)/shard_map/dot_general | solution.py:123
  186.4 1.3 convolution_convert_fusion.1
  187.8 95.8 %all_to_all.29 = bf16[32,32,2048]{2,1,0:T(8,128)(2,1)S(1)} all-to-all(bf16[32,32,2048]{2,1,0:T(8,128)(2,1)S(1)} %bitcast.103), channel_id=1, replica_groups=mesh['sp'=8,'tp'=4] {'sp','tp'}, dimensions={0} | all-to-all | bytes 8388608 | tf_op jit(solution)/shard_map/all_to_all | solution.py:157
  283.6 2.0 copy-done.2
  285.6 2.3 convolution_bitcast_fusion.2
  287.9 9.1 %convolution_convert_fusion = bf16[32,32,2048]{2,1,0:T(8,128)(2,1)} fusion(bf16[32,32,2048]{2,1,0:T(8,128)(2,1)} %copy-done.2, bf16[1,256,2048]{2,1,0:T(8,128)(2,1)S(1)} %copy-done, bf16[1,2048,256]{2,1,0:T(8,128)(2,1)} %param.29, f32[32,1,32,256]{3,2,0,1:T(8,128)} %convolution_bitcast_fusion.2), kind=kOutput, calls=%fused_computation.23 | convolution fusion | flops 2151153664 | bytes 11534336 | tf_op jit(solution)/shard_map/secf,efh->sech/dot_general | solution.py:55
  297.0 4.0 all-to-all-start.2
  301.3 0.4 fusion.75
  301.7 93.0 %all-to-all-done.2 = bf16[32,32,2048]{2,1,0:T(8,128)(2,1)} async-done(((bf16[32,32,2048]{2,1,0:T(8,128)(2,1)}), bf16[32,32,2048]{2,1,0:T(8,128)(2,1)}, u32[]{:S(2)}, u32[]{:S(2)}) %all-to-all-start.2) | async-done | bytes 4194336 | tf_op jit(solution)/shard_map/all_to_all | solution.py:162
  394.7 8.0 %gather_fusion = bf16[512,2048]{1,0:T(8,128)(2,1)} fusion(bf16[1024,2048]{1,0:T(8,128)(2,1)} %bitcast.29, s32[1024]{0:T(1024)S(1)} %pad_clamp_fusion), kind=kCustom, calls=%fused_computation | custom fusion | bytes 4196352 | tf_op jit(solution)/shard_map/gather | solution.py:165
  402.7 4.2 reshape.478
  406.9 3.8 fusion.76
  410.7 3.3 fusion.19
  (77 shorter events, 2.2 us)
Async XLA Ops:
  6.5 281.3 %copy-start = (bf16[1,256,2048]{2,1,0:T(8,128)(2,1)S(1)}, bf16[1,256,2048]{2,1,0:T(8,128)(2,1)}, u32[]{:S(2)}) copy-start(bf16[1,256,2048]{2,1,0:T(8,128)(2,1)} %param.30) | copy-start | bytes 3145732
  6.5 7.9 %copy-start.9 = (f32[128]{0:T(128)S(1)}, f32[128]{0:T(128)}, u32[]{:S(2)}) copy-start(f32[128]{0:T(128)} %param.23) | copy-start | bytes 1540
  6.5 45.6 %all-gather.6.cloned.1.call-start = ((), (), s32[]{:S(2)}) async-start(), calls=%async_computation.4 | async-start | bytes 1179648 | tf_op jit(solution)/shard_map/all_gather | solution.py:92
  9.7 83.8 %all-gather.4.cloned.1.call-start = ((), (), s32[]{:S(2)}) async-start(), calls=%async_computation.3 | async-start | bytes 1179648 | tf_op jit(solution)/shard_map/all_gather | solution.py:93
  15.2 3.5 copy-start.7
  97.2 3.4 copy-start.1
  106.4 3.4 copy-start.1
  115.6 3.4 copy-start.1
  124.8 3.4 copy-start.1
  134.0 3.4 copy-start.1
  143.3 3.4 copy-start.1
  152.5 3.4 copy-start.1
  161.7 3.4 copy-start.1
  167.3 14.3 %copy-start.5 = (bf16[128,2048]{1,0:T(8,128)(2,1)S(1)}, bf16[128,2048]{1,0:T(8,128)(2,1)}, u32[]{:S(2)}) copy-start(bf16[128,2048]{1,0:T(8,128)(2,1)} %param.21) | copy-start | bytes 1572868
  169.1 12.3 %all-to-all-start = ((bf16[4,128,512]{2,1,0:T(8,128)(2,1)}), bf16[4,128,512]{2,1,0:T(8,128)(2,1)S(1)}, u32[]{:S(2)}, u32[]{:S(2)}) async-start(bf16[4,128,512]{2,1,0:T(8,128)(2,1)} %all_to_all.20), calls=%async_computation | async-start | bytes 1048576 | tf_op jit(solution)/shard_map/all_to_all | solution.py:122
  181.6 4.8 %copy-start.6 = (f32[2048]{0:T(1024)S(1)}, f32[2048]{0:T(1024)}, u32[]{:S(2)}) copy-start(f32[2048]{0:T(1024)} %param.25) | copy-start | bytes 24580
  187.7 97.8 %copy-start.10 = (bf16[1,2048,256]{2,1,0:T(8,128)(2,1)S(1)}, bf16[1,2048,256]{2,1,0:T(8,128)(2,1)}, u32[]{:S(2)}) copy-start(bf16[1,2048,256]{2,1,0:T(8,128)(2,1)} %param.28) | copy-start | bytes 3145732
  283.6 2.0 copy-start.2
  297.0 4.1 copy-start.8
  297.0 4.3 %copy-start.4 = (bf16[2048,256]{1,0:T(8,128)(2,1)S(1)}, bf16[2048,256]{1,0:T(8,128)(2,1)}, u32[]{:S(2)}) copy-start(bf16[2048,256]{1,0:T(8,128)(2,1)} %param.31) | copy-start | bytes 3145732
  297.0 97.7 %all-to-all-start.2 = ((bf16[32,32,2048]{2,1,0:T(8,128)(2,1)}), bf16[32,32,2048]{2,1,0:T(8,128)(2,1)}, u32[]{:S(2)}, u32[]{:S(2)}) async-start(bf16[32,32,2048]{2,1,0:T(8,128)(2,1)} %convolution_convert_fusion), calls=%async_computation.2 | async-start | bytes 8388608 | tf_op jit(solution)/shard_map/all_to_all | solution.py:162
  402.7 8.0 %copy-start.3 = (bf16[256,2048]{1,0:T(8,128)(2,1)S(1)}, bf16[256,2048]{1,0:T(8,128)(2,1)}, u32[]{:S(2)}) copy-start(bf16[256,2048]{1,0:T(8,128)(2,1)} %param.33) | copy-start | bytes 3145732
Sparse Core Ops, SparseCore 0:
  9.9 42.2 all-gather.5
  54.2 39.2 all-gather.3
where the time goes:
time: 422 us; the launch traced here: 421 us
  waiting for transfers between devices  176 us (42%)
  blocking collectives  95.8 us (23%)
  matrix products  71 us (17%)
  other arithmetic  34.1 us (8%)
  local copies, waits for them, and re-layouts  21.8 us (5%)
  between operations  13.7 us (3%)
  starting transfers between devices  7.71 us (2%)
    all_to_all x1, blocking collectives, body(): lax.all_to_all(send_rows, ('sp', 'tp'), split_axis=0, concat_axis=0, tile...  95.8 us
    all_to_all x1, waiting for transfers between devices, body(): lax.all_to_all(processed, ('sp', 'tp'), split_axis=0, concat_axis=0, tile...  93 us
    all_gather x1, waiting for transfers between devices, body(): value_piece = lax.all_gather(values, 'sp', axis=0, tiled=True)  41.4 us
    all_gather x1, waiting for transfers between devices, body(): key_piece = lax.all_gather(k_rot, 'sp', axis=0, tiled=True)  32.9 us
    dot_general x8, matrix products, one_block(): jnp.einsum('gqd,kgd->gqk', query_3d, key_3d, preferred_element_type=jnp.f...  28.8 us
    reduce_sum x8, other arithmetic, one_block(): new_sum = running_sum * factor + jnp.sum(weights, axis=-1)  24.4 us
    dot_general x8, matrix products, one_block(): jnp.einsum('gqk,kgd->gqd', weights.astype(jnp.bfloat16), value_3d, prefer...  17.1 us
    dot_general x1, matrix products, expert_apply(): jnp.einsum('secf,efh->sech', hidden_e, expert_down, preferred_element_typ...  9.08 us
  transfers between devices with their start and end apart: 4, of which 4 were waited for; matrix products, arithmetic and copies ran while one was open for 2% of the time, Pallas kernels for 0%

commit v1 on v0

--- a/solution.py
+++ b/solution.py
@@ -9,6 +9,19 @@
 GRID_W = 64
 EPS = 1e-06
 THETA = 10000.0
+
+
+def _save_values(axis_name, obj):
+    degree = lax.axis_size(axis_name)
+    all_blocks = list(map(lambda it: (it, (it + 1) % degree), range(degree)))
+
+    def lift_the_task(block_last):
+        if len(block_last) == degree:
+            return block_last
+        return lift_the_task([lax.ppermute(block_last[0], axis_name, all_blocks), *block_last])
+
+    p_next = jnp.concatenate(lift_the_task([obj]), axis=0)
+    return jnp.roll(p_next, (lax.axis_index(axis_name) + 1) * obj.shape[0], axis=0)
 
 
 def rotate_pairs(block, cosine, sine):
@@ -89,7 +102,7 @@
         jnp.zeros((kv_local, group * tok_local), jnp.float32),
         jnp.zeros((kv_local, group * tok_local, width), jnp.float32),
     )
-    key_piece = lax.all_gather(k_rot, "sp", axis=0, tiled=True)
+    key_piece = _save_values("sp", k_rot)
     value_piece = lax.all_gather(values, "sp", axis=0, tiled=True)
     count = key_piece.shape[0]
     block = math.gcd(count, 512)

time: 422 us -> 404 us (0.957)
  waiting for transfers between devices: 176 us -> 147 us
  local copies, waits for them, and re-layouts: 21.8 us -> 30.6 us
    ppermute x0 -> x7, waiting for transfers between devices: none -> 45.3 us  [lift_the_task(): lax.ppermute(block_last[0], axis_name, all_blocks)]
    all_gather x1, waiting for transfers between devices: 41.4 us -> 0.01 us  [body(): value_piece = lax.all_gather(values, 'sp', axis=0, tiled=True)]
    all_gather x1 -> x0, waiting for transfers between devices: 32.9 us -> none  [body(): key_piece = lax.all_gather(k_rot, 'sp', axis=0, tiled=True)]
    unnamed x23 -> x59, local copies, waits for them, and re-layouts: 3.38 us -> 11.2 us
  transfers between devices with their start and end apart: 4 -> 10, of which waited for: 4 -> 9; matrix products, arithmetic and copies ran while one was open for 2% -> 5% of each run, Pallas kernels for 0% -> 0%
where the time goes in v1:
time: 404 us; the launch traced here: 403 us
  waiting for transfers between devices  147 us (36%)
  blocking collectives  95.5 us (24%)
  matrix products  71.7 us (18%)
  other arithmetic  34.3 us (8%)
  local copies, waits for them, and re-layouts  30.6 us (8%)
  between operations  14 us (3%)
  starting transfers between devices  10.3 us (3%)
    all_to_all x1, blocking collectives, body(): lax.all_to_all(send_rows, ('sp', 'tp'), split_axis=0, concat_axis=0, tile...  95.5 us
    all_to_all x1, waiting for transfers between devices, body(): lax.all_to_all(processed, ('sp', 'tp'), split_axis=0, concat_axis=0, tile...  93 us
    ppermute x7, waiting for transfers between devices, lift_the_task(): lax.ppermute(block_last[0], axis_name, all_blocks)  45.3 us
    dot_general x8, matrix products, one_block(): jnp.einsum('gqd,kgd->gqk', query_3d, key_3d, preferred_element_type=jnp.f...  28.7 us
    reduce_sum x8, other arithmetic, one_block(): new_sum = running_sum * factor + jnp.sum(weights, axis=-1)  24.4 us
    dot_general x8, matrix products, one_block(): jnp.einsum('gqk,kgd->gqd', weights.astype(jnp.bfloat16), value_3d, prefer...  17.1 us
    unnamed x59, local copies, waits for them, and re-layouts  11.2 us
    dot_general x1, matrix products, expert_apply(): jnp.einsum('secf,efh->sech', hidden_e, expert_down, preferred_element_typ...  9.08 us
  transfers between devices with their start and end apart: 10, of which 9 were waited for; matrix products, arithmetic and copies ran while one was open for 5% of the time, Pallas kernels for 0%

profile of v1, /device:TPU:0, one launch (start us, length us, event | category | flops | bytes accessed | tf_op | source)
XLA Modules:
  0.0 403.3 jit_solution(7338043587615326091)
XLA Ops:
  6.6 1.1 copy.35
  9.7 3.0 collective-permute-start
  12.8 1.4 reshape.480
  14.2 5.1 %collective-permute-done = bf16[512,128]{0,1:T(8,128)(2,1)S(1)} collective-permute-done((bf16[512,128]{0,1:T(8,128)(2,1)S(1)}, bf16[512,128]{0,1:T(8,128)(2,1)S(1)}, u32[]{:S(2)}, u32[]{:S(2)}) %collective-permute-start) | collective-permute-done | bytes 131104 | tf_op jit(solution)/shard_map/ppermute | solution.py:21
  19.9 7.5 %collective-permute-done.1 = bf16[512,128]{0,1:T(8,128)(2,1)S(1)} collective-permute-done((bf16[512,128]{0,1:T(8,128)(2,1)S(1)}, bf16[512,128]{0,1:T(8,128)(2,1)S(1)}, u32[]{:S(2)}, u32[]{:S(2)}) %collective-permute-start.1) | collective-permute-done | bytes 131104 | tf_op jit(solution)/shard_map/ppermute | solution.py:21
  27.5 8.3 %collective-permute-done.2 = bf16[512,128]{0,1:T(8,128)(2,1)S(1)} collective-permute-done((bf16[512,128]{0,1:T(8,128)(2,1)S(1)}, bf16[512,128]{0,1:T(8,128)(2,1)S(1)}, u32[]{:S(2)}, u32[]{:S(2)}) %collective-permute-start.2) | collective-permute-done | bytes 131104 | tf_op jit(solution)/shard_map/ppermute | solution.py:21
  36.5 7.1 %collective-permute-done.3 = bf16[512,128]{0,1:T(8,128)(2,1)S(1)} collective-permute-done((bf16[512,128]{0,1:T(8,128)(2,1)S(1)}, bf16[512,128]{0,1:T(8,128)(2,1)S(1)}, u32[]{:S(2)}, u32[]{:S(2)}) %collective-permute-start.3) | collective-permute-done | bytes 131104 | tf_op jit(solution)/shard_map/ppermute | solution.py:21
  43.6 1.9 multiply_cosine_fusion.1
  45.5 6.9 %collective-permute-done.4 = bf16[512,128]{0,1:T(8,128)(2,1)S(1)} collective-permute-done((bf16[512,128]{0,1:T(8,128)(2,1)S(1)}, bf16[512,128]{0,1:T(8,128)(2,1)S(1)}, u32[]{:S(2)}, u32[]{:S(2)}) %collective-permute-start.4) | collective-permute-done | bytes 131104 | tf_op jit(solution)/shard_map/ppermute | solution.py:21
  52.3 1.8 fusion.37
  54.2 6.0 %collective-permute-done.5 = bf16[512,128]{0,1:T(8,128)(2,1)} collective-permute-done((bf16[512,128]{0,1:T(8,128)(2,1)S(1)}, bf16[512,128]{0,1:T(8,128)(2,1)}, u32[]{:S(2)}, u32[]{:S(2)}) %collective-permute-start.5) | collective-permute-done | bytes 131104 | tf_op jit(solution)/shard_map/ppermute | solution.py:21
  60.1 1.6 maximum_bitcast_fusion
  61.9 0.8 copy.42
  62.8 0.9 fusion.25
  63.7 4.4 %collective-permute-done.6 = bf16[512,128]{0,1:T(8,128)(2,1)} collective-permute-done((bf16[512,128]{0,1:T(8,128)(2,1)}, bf16[512,128]{0,1:T(8,128)(2,1)}, u32[]{:S(2)}, u32[]{:S(2)}) %collective-permute-start.6) | collective-permute-done | bytes 131104 | tf_op jit(solution)/shard_map/ppermute | solution.py:21
  68.1 0.9 constant_dynamic-update-slice_fusion.15
  69.0 0.9 constant_dynamic-update-slice_fusion.14
  69.9 0.9 constant_dynamic-update-slice_fusion.13
  70.8 0.9 constant_dynamic-update-slice_fusion.12
  71.8 0.8 constant_dynamic-update-slice_fusion.8
  72.6 0.9 constant_dynamic-update-slice_fusion.7
  73.6 0.9 constant_dynamic-update-slice_fusion.6
  74.5 0.9 constant_dynamic-update-slice_fusion.5
  75.5 1.1 constant_dynamic-slice_fusion
  76.6 73.8 %while.18 = (s32[]{:T(128)}, f32[1,2048]{1,0:T(1,128)S(1)}, f32[1,2048]{1,0:T(1,128)S(1)}, f32[1,2048,128]{2,1,0:T(8,128)S(1)}, bf16[4096,128]{0,1:T(8,128)(2,1)...) while((s32[]{:T(128)}, f32[1,2048]{1,0:T(1,128)S(1)}, ...), condition=%wide.region_5.6_spmd.clone, body=%wide.region_2.5_spmd.clone.sunk | while | flops 546056192 | bytes 32374992 | solution.py:131
  76.6 3.6 multiply_reduce_fusion.4
  80.2 3.0 fusion.96
  83.7 2.1 fusion.98
  85.8 3.6 multiply_reduce_fusion.4
  89.5 3.0 fusion.96
  92.9 2.1 fusion.98
  95.1 3.6 multiply_reduce_fusion.4
  98.7 3.0 fusion.96
  102.1 2.1 fusion.98
  104.3 3.6 multiply_reduce_fusion.4
  107.9 3.0 fusion.96
  111.3 2.1 fusion.98
  113.5 3.6 multiply_reduce_fusion.4
  117.1 3.0 fusion.96
  120.6 2.1 fusion.98
  122.7 3.6 multiply_reduce_fusion.4
  126.3 3.0 fusion.96
  129.8 2.1 fusion.98
  132.0 3.6 multiply_reduce_fusion.4
  135.6 3.0 fusion.96
  139.0 2.1 fusion.98
  141.2 3.6 multiply_reduce_fusion.4
  144.8 3.0 fusion.96
  148.2 2.1 fusion.98
  151.2 1.0 all_to_all.20
  152.2 3.5 all-to-all-start
  156.1 8.3 %all-to-all-done = bf16[4,128,512]{2,1,0:T(8,128)(2,1)S(1)} async-done(((bf16[4,128,512]{2,1,0:T(8,128)(2,1)}), bf16[4,128,512]{2,1,0:T(8,128)(2,1)S(1)}, u32[]{:S(2)}, u32[]{:S(2)}) %all-to-all-start) | async-done | bytes 524320 | tf_op jit(solution)/shard_map/all_to_all | solution.py:135
  164.7 4.7 %multiply_reduce_fusion.1 = (f32[128]{0:T(128)S(1)}, f32[128,2048]{1,0:T(8,128)S(1)}) fusion(bf16[128,2048]{0,1:T(8,128)(2,1)S(1)} %bitcast.111, bf16[2048,2048]{1,0:T(8,128)(2,1)} %param.22, bf16[128,2048]{1,0:T(8,128)(2,1)S(1)} %copy-done.5), kind=kOutput, calls=%fused_computation.52 | convolution fusion | flops 1075314560 | bytes 10486272 | tf_op jit(solution)/shard_map/dot_general | solution.py:136
  169.5 1.3 convolution_convert_fusion.1
  170.8 95.5 %all_to_all.29 = bf16[32,32,2048]{2,1,0:T(8,128)(2,1)S(1)} all-to-all(bf16[32,32,2048]{2,1,0:T(8,128)(2,1)S(1)} %bitcast.108), channel_id=1, replica_groups=mesh['sp'=8,'tp'=4] {'sp','tp'}, dimensions={0} | all-to-all | bytes 8388608 | tf_op jit(solution)/shard_map/all_to_all | solution.py:170
  266.3 2.0 copy-done.2
  268.3 2.3 convolution_bitcast_fusion.2
  270.7 9.1 %convolution_convert_fusion = bf16[32,32,2048]{2,1,0:T(8,128)(2,1)} fusion(bf16[32,32,2048]{2,1,0:T(8,128)(2,1)} %copy-done.2, bf16[1,256,2048]{2,1,0:T(8,128)(2,1)S(1)} %copy-done, bf16[1,2048,256]{2,1,0:T(8,128)(2,1)} %param.29, f32[32,1,32,256]{3,2,0,1:T(8,128)} %convolution_bitcast_fusion.2), kind=kOutput, calls=%fused_computation.23 | convolution fusion | flops 2151153664 | bytes 11534336 | tf_op jit(solution)/shard_map/secf,efh->sech/dot_general | solution.py:68
  279.7 3.7 all-to-all-start.2
  284.1 93.0 %all-to-all-done.2 = bf16[32,32,2048]{2,1,0:T(8,128)(2,1)} async-done(((bf16[32,32,2048]{2,1,0:T(8,128)(2,1)}), bf16[32,32,2048]{2,1,0:T(8,128)(2,1)}, u32[]{:S(2)}, u32[]{:S(2)}) %all-to-all-start.2) | async-done | bytes 4194336 | tf_op jit(solution)/shard_map/all_to_all | solution.py:175
  377.2 8.0 %gather_fusion = bf16[512,2048]{1,0:T(8,128)(2,1)} fusion(bf16[1024,2048]{1,0:T(8,128)(2,1)} %bitcast.29, s32[1024]{0:T(1024)S(1)} %pad_clamp_fusion), kind=kCustom, calls=%fused_computation | custom fusion | bytes 4196352 | tf_op jit(solution)/shard_map/gather | solution.py:178
  385.1 4.1 %reshape.478 = bf16[128,4,2048]{2,1,0:T(4,128)(2,1)} reshape(bf16[512,2048]{1,0:T(8,128)(2,1)} %gather_fusion) | data formatting | bytes 4194304 | tf_op jit(solution)/shard_map/reshape | solution.py:178
  389.2 3.9 fusion.76
  393.1 3.3 fusion.19
  (127 shorter events, 9.0 us)
Async XLA Ops:
  6.5 264.1 %copy-start = (bf16[1,256,2048]{2,1,0:T(8,128)(2,1)S(1)}, bf16[1,256,2048]{2,1,0:T(8,128)(2,1)}, u32[]{:S(2)}) copy-start(bf16[1,256,2048]{2,1,0:T(8,128)(2,1)} %param.30) | copy-start | bytes 3145732
  6.5 70.1 %all-gather.2.cloned.1.call-start = ((), (), s32[]{:S(2)}) async-start(), calls=%async_computation.3 | async-start | bytes 1179648 | tf_op jit(solution)/shard_map/all_gather | solution.py:106
  8.5 27.3 %copy-start.20 = (f32[128]{0:T(128)S(1)}, f32[128]{0:T(128)}, u32[]{:S(2)}) copy-start(f32[128]{0:T(128)} %param.23) | copy-start | bytes 1540
  9.1 0.6 copy-start.9
  9.1 0.6 copy-start.11
  9.1 0.6 copy-start.13
  9.1 0.6 copy-start.15
  9.7 9.6 %collective-permute-start = (bf16[512,128]{0,1:T(8,128)(2,1)S(1)}, bf16[512,128]{0,1:T(8,128)(2,1)S(1)}, u32[]{:S(2)}, u32[]{:S(2)}) collective-permute-start(bf16[512,128]{0,1:T(8,128)(2,1)S(1)} %maximum_bitcast_fusion.1), channel_id=1, source_target_pairs={{0,4},{4,8},{8,12},{12,16},{16,20},{20,24},{24,28},{28,0},{1,5},{5... | collective-permute-start | bytes 393224 | tf_op jit(solution)/shard_map/ppermute | solution.py:21
  19.3 8.1 %collective-permute-start.1 = (bf16[512,128]{0,1:T(8,128)(2,1)S(1)}, bf16[512,128]{0,1:T(8,128)(2,1)S(1)}, u32[]{:S(2)}, u32[]{:S(2)}) collective-permute-start(bf16[512,128]{0,1:T(8,128)(2,1)S(1)} %collective-permute-done), channel_id=1, source_target_pairs={{0,4},{4,8},{8,12},{12,16},{16,20},{20,24},{24,28},{28,0},{1,5},{5... | collective-permute-start | bytes 393224 | tf_op jit(solution)/shard_map/ppermute | solution.py:21
  27.5 8.4 %collective-permute-start.2 = (bf16[512,128]{0,1:T(8,128)(2,1)S(1)}, bf16[512,128]{0,1:T(8,128)(2,1)S(1)}, u32[]{:S(2)}, u32[]{:S(2)}) collective-permute-start(bf16[512,128]{0,1:T(8,128)(2,1)S(1)} %collective-permute-done.1), channel_id=1, source_target_pairs={{0,4},{4,8},{8,12},{12,16},{16,20},{20,24},{24,28},{28,0},{1,5},{5... | collective-permute-start | bytes 393224 | tf_op jit(solution)/shard_map/ppermute | solution.py:21
  35.8 7.8 %collective-permute-start.3 = (bf16[512,128]{0,1:T(8,128)(2,1)S(1)}, bf16[512,128]{0,1:T(8,128)(2,1)S(1)}, u32[]{:S(2)}, u32[]{:S(2)}) collective-permute-start(bf16[512,128]{0,1:T(8,128)(2,1)S(1)} %collective-permute-done.2), channel_id=1, source_target_pairs={{0,4},{4,8},{8,12},{12,16},{16,20},{20,24},{24,28},{28,0},{1,5},{5... | collective-permute-start | bytes 393224 | tf_op jit(solution)/shard_map/ppermute | solution.py:21
  43.6 10.5 %copy-start.6 = (bf16[512,128]{0,1:T(8,128)(2,1)}, bf16[512,128]{0,1:T(8,128)(2,1)S(1)}, u32[]{:S(2)}) copy-start(bf16[512,128]{0,1:T(8,128)(2,1)S(1)} %collective-permute-done.3) | copy-start | bytes 393220
  43.6 8.7 %collective-permute-start.4 = (bf16[512,128]{0,1:T(8,128)(2,1)S(1)}, bf16[512,128]{0,1:T(8,128)(2,1)S(1)}, u32[]{:S(2)}, u32[]{:S(2)}) collective-permute-start(bf16[512,128]{0,1:T(8,128)(2,1)S(1)} %collective-permute-done.3), channel_id=1, source_target_pairs={{0,4},{4,8},{8,12},{12,16},{16,20},{20,24},{24,28},{28,0},{1,5},{5... | collective-permute-start | bytes 393224 | tf_op jit(solution)/shard_map/ppermute | solution.py:21
  52.3 1.8 copy-start.8
  52.3 7.8 %collective-permute-start.5 = (bf16[512,128]{0,1:T(8,128)(2,1)S(1)}, bf16[512,128]{0,1:T(8,128)(2,1)}, u32[]{:S(2)}, u32[]{:S(2)}) collective-permute-start(bf16[512,128]{0,1:T(8,128)(2,1)S(1)} %collective-permute-done.4), channel_id=1, source_target_pairs={{0,4},{4,8},{8,12},{12,16},{16,20},{20,24},{24,28},{28,0},{1,5},{5... | collective-permute-start | bytes 393224 | tf_op jit(solution)/shard_map/ppermute | solution.py:21
  60.1 8.0 %collective-permute-start.6 = (bf16[512,128]{0,1:T(8,128)(2,1)}, bf16[512,128]{0,1:T(8,128)(2,1)}, u32[]{:S(2)}, u32[]{:S(2)}) collective-permute-start(bf16[512,128]{0,1:T(8,128)(2,1)} %collective-permute-done.5), channel_id=1, source_target_pairs={{0,4},{4,8},{8,12},{12,16},{16,20},{20,24},{24,28},{28,0},{1,5},{5... | collective-permute-start | bytes 393224 | tf_op jit(solution)/shard_map/ppermute | solution.py:21
  61.8 13.6 %copy-start.7 = (bf16[512,128]{0,1:T(8,128)(2,1)S(1)}, bf16[512,128]{0,1:T(8,128)(2,1)}, u32[]{:S(2)}) copy-start(bf16[512,128]{0,1:T(8,128)(2,1)} %copy-done.6) | copy-start | bytes 393220
  62.8 12.7 %copy-start.10 = (bf16[512,1,32]{0,2,1:T(8,128)(2,1)S(1)}, bf16[512,1,32]{0,2,1:T(8,128)(2,1)}, u32[]{:S(2)}) copy-start(bf16[512,1,32]{0,2,1:T(8,128)(2,1)} %copy-done.9) | copy-start | bytes 98308
  62.8 12.7 %copy-start.12 = (bf16[512,1,32]{0,2,1:T(8,128)(2,1)S(1)}, bf16[512,1,32]{0,2,1:T(8,128)(2,1)}, u32[]{:S(2)}) copy-start(bf16[512,1,32]{0,2,1:T(8,128)(2,1)} %copy-done.11) | copy-start | bytes 98308
  62.8 12.7 %copy-start.14 = (bf16[512,1,32]{0,2,1:T(8,128)(2,1)S(1)}, bf16[512,1,32]{0,2,1:T(8,128)(2,1)}, u32[]{:S(2)}) copy-start(bf16[512,1,32]{0,2,1:T(8,128)(2,1)} %copy-done.13) | copy-start | bytes 98308
  62.8 12.7 %copy-start.16 = (bf16[512,1,32]{0,2,1:T(8,128)(2,1)S(1)}, bf16[512,1,32]{0,2,1:T(8,128)(2,1)}, u32[]{:S(2)}) copy-start(bf16[512,1,32]{0,2,1:T(8,128)(2,1)} %copy-done.15) | copy-start | bytes 98308
  80.2 3.5 copy-start.1
  89.4 3.5 copy-start.1
  98.7 3.5 copy-start.1
  107.9 3.5 copy-start.1
  117.1 3.5 copy-start.1
  126.3 3.5 copy-start.1
  135.6 3.5 copy-start.1
  144.8 3.5 copy-start.1
  150.4 5.3 %copy-start.19 = (f32[512]{0:T(512)S(1)}, f32[512]{0:T(512)}, u32[]{:S(2)}) copy-start(f32[512]{0:T(512)} %fusion.25) | copy-start | bytes 6148
  151.2 13.5 %copy-start.5 = (bf16[128,2048]{1,0:T(8,128)(2,1)S(1)}, bf16[128,2048]{1,0:T(8,128)(2,1)}, u32[]{:S(2)}) copy-start(bf16[128,2048]{1,0:T(8,128)(2,1)} %param.21) | copy-start | bytes 1572868
  152.2 12.3 %all-to-all-start = ((bf16[4,128,512]{2,1,0:T(8,128)(2,1)}), bf16[4,128,512]{2,1,0:T(8,128)(2,1)S(1)}, u32[]{:S(2)}, u32[]{:S(2)}) async-start(bf16[4,128,512]{2,1,0:T(8,128)(2,1)} %all_to_all.20), calls=%async_computation | async-start | bytes 1048576 | tf_op jit(solution)/shard_map/all_to_all | solution.py:135
  164.7 4.8 %copy-start.17 = (f32[2048]{0:T(1024)S(1)}, f32[2048]{0:T(1024)}, u32[]{:S(2)}) copy-start(f32[2048]{0:T(1024)} %param.25) | copy-start | bytes 24580
  170.8 97.5 %copy-start.21 = (bf16[1,2048,256]{2,1,0:T(8,128)(2,1)S(1)}, bf16[1,2048,256]{2,1,0:T(8,128)(2,1)}, u32[]{:S(2)}) copy-start(bf16[1,2048,256]{2,1,0:T(8,128)(2,1)} %param.28) | copy-start | bytes 3145732
  266.3 2.0 copy-start.2
  279.7 3.8 copy-start.18
  279.7 4.0 %copy-start.4 = (bf16[2048,256]{1,0:T(8,128)(2,1)S(1)}, bf16[2048,256]{1,0:T(8,128)(2,1)}, u32[]{:S(2)}) copy-start(bf16[2048,256]{1,0:T(8,128)(2,1)} %param.31) | copy-start | bytes 3145732
  279.7 97.4 %all-to-all-start.2 = ((bf16[32,32,2048]{2,1,0:T(8,128)(2,1)}), bf16[32,32,2048]{2,1,0:T(8,128)(2,1)}, u32[]{:S(2)}, u32[]{:S(2)}) async-start(bf16[32,32,2048]{2,1,0:T(8,128)(2,1)} %convolution_convert_fusion), calls=%async_computation.2 | async-start | bytes 8388608 | tf_op jit(solution)/shard_map/all_to_all | solution.py:175
  389.2 3.9 copy-start.3
Sparse Core Ops, SparseCore 0:
  12.9 43.9 all-gather.1
